TPU v7x, 32 devices: a whole 2x2x4 slice. The times are simulated.
32 devices in a mesh: sp: 8 (over z, x), tp: 4 (over y, core).
Axes of the slice: x: 2, y: 2, z: 4, core: 2. Of those that a mesh axis runs over, the one named last changes fastest.
Arguments:
- tokens: bfloat16 [3072, 2048], P('sp', 'tp'), may hold values from -6 to 6
- pre_gain: float32 [2048], replicated, may hold values from 0.1 to 1.9
- outer_gate_weight: bfloat16 [2048, 1024], P(None, 'tp'), may hold values from -0.125 to 0.125
- inner_gate_weight: bfloat16 [2048, 1024], P(None, 'tp'), may hold values from -0.125 to 0.125
- source_weight: bfloat16 [2048, 1024], P(None, 'tp'), may hold values from -0.125 to 0.125
- conv_taps: bfloat16 [3, 1024], P(None, 'tp'), may hold values from -3.5 to 3.5
- q_down_weight: bfloat16 [2048, 768], replicated, may hold values from -0.125 to 0.125
- q_norm_gain: float32 [768], replicated, may hold values from 0.5 to 16
- q_up_weight: bfloat16 [768, 3072], P(None, 'tp'), may hold values from -0.21875 to 0.21875
- kv_down_weight: bfloat16 [2048, 512], replicated, may hold values from -0.125 to 0.125
- rope_key_weight: bfloat16 [2048, 32], replicated, may hold values from -0.125 to 0.125
- kv_norm_gain: float32 [512], replicated, may hold values from 0.5 to 16
- kv_up_weight: bfloat16 [512, 4096], P(None, 'tp'), may hold values from -0.25 to 0.25
- attn_out_weight: bfloat16 [2048, 2048], P('tp'), may hold values from -4 to 4
- conv_out_weight: bfloat16 [1024, 2048], P('tp'), may hold values from -0.1875 to 0.1875
- post_gain: float32 [2048], P('tp'), may hold values from 0.1 to 1.9
Outputs:
- mixed: bfloat16 [3072, 2048], P('sp', 'tp')
- log_total: float32 [32, 3072], P('tp', 'sp')
All inputs are finite; a program needn't handle non-finite values.
Results may differ from a plain program's by a relative error of at most 0.017.
The roundings to bfloat16 on the way count: a program that leaves them out, or rounds other values in their place, can miss the bound.
Values may be sent and summed in bfloat16 or wider, within the bound.
A program may use at most 128 MiB of HBM per device.

v0:
```python
import jax
import jax.numpy as jnp
from jax import lax
from jax.sharding import PartitionSpec as P

D = 2048
NOPE = 64
ROPE = 32
VDIM = 64
TAPS = 3


EPSILON = 1e-06
THETA = 500000.0
NEGATIVE = -1e30


def from_behind(value, axis, steps):
    count = lax.axis_size(axis)
    leading, last = (max(0, -steps), min(count, count - steps))
    return lax.ppermute(value, axis, [(source, source + steps) for source in range(leading, last)])


def rms_factor(values):
    return lax.rsqrt(jnp.mean(values * values, axis=-1, keepdims=True) + EPSILON)


def rotation(positions, width):
    freqs = THETA ** (-jnp.arange(0, width, 2, dtype=jnp.float32) / width)
    angles = positions.astype(jnp.float32)[:, None] * freqs[None, :]
    return (jnp.cos(angles), jnp.sin(angles))


def rotate(values, cosine, sine):
    half = values.shape[-1] // 2
    first = values[..., :half]
    second = values[..., half:]
    return jnp.concatenate(
        [first * cosine - second * sine, second * cosine + first * sine], axis=-1
    )


def block_count(rows):
    count = 1
    while rows // count > 1024 or rows % count != 0:
        count += 1
    return count


def attend(
    state, query_plain, query_turned, key_plain, values, key_turned, key_start, query_pos, scale
):
    maxima, totals, weighted = state
    rows = key_plain.shape[0]
    scores = jnp.einsum("thd,nhd->htn", query_plain, key_plain, preferred_element_type=jnp.float32)
    scores = scores + jnp.einsum(
        "thr,nr->htn", query_turned, key_turned, preferred_element_type=jnp.float32
    )
    key_pos = key_start + jnp.arange(rows, dtype=jnp.int32)
    allowed = key_pos[None, :] <= query_pos[:, None]
    scores = jnp.where(allowed[None], scores * scale, NEGATIVE)
    fresh = jnp.maximum(maxima, jnp.max(scores, axis=-1))
    shrink = jnp.exp(maxima - fresh)
    weights = jnp.exp(scores - fresh[..., None])
    totals = totals * shrink + jnp.sum(weights, axis=-1)
    weighted = weighted * shrink[..., None] + jnp.einsum(
        "htn,nhd->htd", weights.astype(jnp.bfloat16), values, preferred_element_type=jnp.float32
    )
    return (fresh, totals, weighted)


def body(
    tokens,
    pre_gain,
    outer_gate_weight,
    inner_gate_weight,
    source_weight,
    conv_taps,
    q_down_weight,
    q_norm_gain,
    q_up_weight,
    kv_down_weight,
    rope_key_weight,
    kv_norm_gain,
    kv_up_weight,
    attn_out_weight,
    conv_out_weight,
    post_gain,
):
    token_rows = tokens.shape[0]
    weights_in = (
        outer_gate_weight,
        inner_gate_weight,
        source_weight,
        q_down_weight,
        kv_down_weight,
        rope_key_weight,
    )
    wide = lax.all_gather(tokens, "tp", axis=1, tiled=True).astype(jnp.float32)
    scaled = (wide * pre_gain).astype(jnp.bfloat16)
    squares = jnp.sum(wide * wide, axis=1)
    sums = tuple(
        (jnp.dot(scaled, weight, preferred_element_type=jnp.float32) for weight in weights_in)
    )
    squares, sums = (squares, sums)
    factor = lax.rsqrt(squares / D + EPSILON)[:, None]
    outer_sum, inner_sum, source_sum, q_sum, kv_sum, rope_sum = sums
    outer = (outer_sum * factor).astype(jnp.bfloat16)
    inner = (inner_sum * factor).astype(jnp.bfloat16)
    source = (source_sum * factor).astype(jnp.bfloat16)
    driven = (inner.astype(jnp.float32) * source.astype(jnp.float32)).astype(jnp.bfloat16)
    prior = from_behind(driven[token_rows - (TAPS - 1) :], "sp", 1)
    extended = jnp.concatenate([prior, driven], axis=0)
    convolved = jnp.zeros(driven.shape, jnp.float32)
    for index in range(TAPS):
        convolved = convolved + conv_taps[index].astype(jnp.float32) * extended[
            index : index + token_rows
        ].astype(jnp.float32)
    conv_branch = (outer.astype(jnp.float32) * convolved).astype(jnp.bfloat16)
    local_heads = q_up_weight.shape[1] // (NOPE + ROPE)
    query_pos = lax.axis_index("sp") * token_rows + jnp.arange(token_rows, dtype=jnp.int32)
    last_pos = lax.axis_index("sp") * token_rows + token_rows - 1
    cosine, sine = rotation(query_pos, ROPE)
    q_latent = q_sum * factor
    q_normed = (q_latent * rms_factor(q_latent) * q_norm_gain).astype(jnp.bfloat16)
    query = jnp.dot(q_normed, q_up_weight, preferred_element_type=jnp.float32)
    query = query.reshape(token_rows, local_heads, NOPE + ROPE)
    q_plain = query[..., :NOPE].astype(jnp.bfloat16)
    q_turned = rotate(query[..., NOPE:], cosine[:, None], sine[:, None]).astype(jnp.bfloat16)
    kv_latent = kv_sum * factor
    latent = (kv_latent * rms_factor(kv_latent) * kv_norm_gain).astype(jnp.bfloat16)
    rope_key = rotate(rope_sum * factor, cosine, sine).astype(jnp.bfloat16)
    scale = (NOPE + ROPE) ** (-0.5)

    def split_keys(flat):
        shaped = flat.reshape(flat.shape[0], local_heads, NOPE + VDIM)
        return (shaped[..., :NOPE], shaped[..., NOPE:])

    start_state = (
        jnp.full((local_heads, token_rows), NEGATIVE, jnp.float32),
        jnp.zeros((local_heads, token_rows), jnp.float32),
        jnp.zeros((local_heads, token_rows, VDIM), jnp.float32),
    )

    def expand_latent(block):
        return split_keys(
            jnp.dot(block, kv_up_weight, preferred_element_type=jnp.float32).astype(jnp.bfloat16)
        )

    pieces = (
        lax.all_gather(latent, "sp", axis=0, tiled=True),
        lax.all_gather(rope_key, "sp", axis=0, tiled=True),
    )
    rows = pieces[0].shape[0]
    count = block_count(rows)
    size = rows // count

    def advance(index, current_state):
        offset = index * size

        def compute(current):
            block = tuple((lax.dynamic_slice_in_dim(member, offset, size, 0) for member in pieces))
            key_plain, values = expand_latent(block[0])
            return attend(
                current, q_plain, q_turned, key_plain, values, block[1], offset, query_pos, scale
            )

        return lax.cond(offset <= last_pos, compute, lambda current: current, current_state)

    final = lax.fori_loop(0, count, advance, start_state)
    maxima, totals, weighted = final
    log_total = maxima + jnp.log(totals)
    attended = (weighted / totals[..., None]).astype(jnp.bfloat16)
    out_rows = attn_out_weight.reshape(local_heads, VDIM, attn_out_weight.shape[1])
    partial_value = jnp.einsum(
        "htd,hdk->tk", attended, out_rows, preferred_element_type=jnp.float32
    )
    partial_value = partial_value + jnp.dot(
        conv_branch, conv_out_weight, preferred_element_type=jnp.float32
    )
    summed = lax.psum_scatter(
        partial_value.astype(jnp.bfloat16), "tp", scatter_dimension=1, tiled=True
    ).astype(jnp.float32)
    row_squares = lax.psum(jnp.sum(summed * summed, axis=1), "tp")
    mixed = summed * lax.rsqrt(row_squares / D + EPSILON)[:, None] * post_gain
    return (mixed.astype(jnp.bfloat16), log_total)


def solution(mesh):
    placed = (
        P("sp", "tp"),
        P(),
        P(None, "tp"),
        P(None, "tp"),
        P(None, "tp"),
        P(None, "tp"),
        P(),
        P(),
        P(None, "tp"),
        P(),
        P(),
        P(),
        P(None, "tp"),
        P("tp", None),
        P("tp", None),
        P("tp"),
    )
    return jax.shard_map(
        body, mesh=mesh, in_specs=placed, out_specs=(P("sp", "tp"), P("tp", "sp")), check_vma=False
    )
```

profile of v0, /device:TPU:27, one launch (start us, length us, event | category | flops | bytes accessed | tf_op | source)
XLA Modules:
  0.0 214.7 jit_solution(13920093443790538715)
XLA Ops:
  8.0 22.6 %all-gather.3.cloned.1.call-done = bf16[384,2048]{1,0:T(8,128)(2,1)} async-done(((bf16[384,512]{1,0:T(8,128)(2,1)}), bf16[384,2048]{1,0:T(8,128)(2,1)}) %all-gather.3.cloned.1.call-update) | async-done | bytes 1572880 | tf_op jit(solution)/shard_map/all_gather | solution.py:99
  32.4 3.2 %multiply_reduce_fusion.1 = (f32[384]{0:T(512)S(1)}, f32[384,512]{1,0:T(8,128)S(1)}) fusion(f32[384]{0:T(512)S(1)} %add_rsqrt_fusion.3, bf16[2048,512]{1,0:T(8,128)(2,1)} %param.29, bf16[384,2048]{1,0:T(8,128)(2,1)} %all-gather.3.cloned.1.call-done, f32[2048]{0:T(1024)} %param.21), kind=kOutput, calls=%fused_computation.56 | convolution fusion | flops 808255104 | bytes 4467712 | tf_op jit(solution)/shard_map/dot_general | solution.py:103
  37.2 3.0 %multiply_reduce_fusion = (f32[384]{0:T(512)S(1)}, f32[384,768]{1,0:T(8,128)S(1)}) fusion(f32[384]{0:T(512)S(1)} %add_rsqrt_fusion.3, bf16[2048,768]{1,0:T(8,128)(2,1)S(1)} %copy-done, bf16[384,2048]{1,0:T(8,128)(2,1)} %all-gather.3.cloned.1.call-done, f32[2048]{0:T(1024)S(1)} %copy-done.11), kind=kOutput, calls=%fused_computation.36 | convolution fusion | flops 1211203200 | bytes 5909504 | tf_op jit(solution)/shard_map/dot_general | solution.py:103
  46.4 27.5 %all_gather.11 = bf16[3072,32]{0,1:T(8,128)(2,1)} all-gather(bf16[384,32]{0,1:T(8,128)(2,1)S(1)} %pad_maximum_fusion.3), channel_id=1, replica_groups=mesh['sp'=8,'tp'=4] {'sp'}, dimensions={0}, use_global_device_ids=true | all-gather | bytes 221184 | tf_op jit(solution)/shard_map/all_gather | solution.py:152
  74.7 21.6 %all-gather.5.cloned.1.call-done = bf16[3072,512]{1,0:T(8,128)(2,1)} async-done(((bf16[384,512]{1,0:T(8,128)(2,1)}), bf16[3072,512]{1,0:T(8,128)(2,1)}) %all-gather.5.cloned.1.call-update) | async-done | bytes 3145744 | tf_op jit(solution)/shard_map/all_gather | solution.py:151
  97.9 62.0 %while.18 = (s32[]{:T(128)}, f32[8,384]{1,0:T(8,128)S(1)}, f32[8,384]{1,0:T(8,128)}, f32[8,384,64]{1,2,0:T(8,128)}, s32[]{:T(128)}, /*index=5*/bf16[3072,512]{1,...) while((s32[]{:T(128)}, f32[8,384]{1,0:T(8,128)S(1)}, ...), condition=%wide.region_8.9_spmd.clone, body=%wide.region_3.8_spmd.clone.sunk | while | flops 2107383168 | bytes 79608296 | solution.py:170
  97.9 20.7 %conditional.3 = ((f32[8,384]{1,0:T(8,128)S(1)}, f32[8,384]{1,0:T(8,128)}, f32[8,384,64]{1,2,0:T(8,128)})) conditional(s32[]{:T(128)} %convert_element_type.206, (f32[8,384]{1,0:T(8,128)S(1)}, f32[8,384]{1,0:T(8,128)}, f32[8,384,64]{1,2,0:T(8,128)}) %tuple.57, (s32[]{:T(128)}, s32[]{:T(128)}, bf16[3072,512]{1,0:T(8,128)(2,1)}, ...), branch_computations={%region_4.0_spmd, %region_5.7_spmd} | conditional | flops 2107383168 | bytes 79606488 | solution.py:168
  97.9 2.8 %convolution_convert_fusion = bf16[1024,1024]{0,1:T(8,128)(2,1)S(1)} fusion(bf16[512,1024]{1,0:T(8,128)(2,1)} %get-tuple-element.207, bf16[3072,512]{1,0:T(8,128)(2,1)} %get-tuple-element.206, s32[]{:T(128)S(6)} %select_n.6), kind=kOutput, calls=%fused_computation.9 | convolution fusion | flops 1074790400 | bytes 4194308 | tf_op jit(solution)/shard_map/while/body/eval_jaxpr/cond/branch_1_fun/dot_general | solution.py:147
  100.8 6.4 %fusion.13 = f32[8,1024,384]{2,1,0:T(8,128)} fusion(bf16[384,8,64]{0,2,1:T(8,128)(2,1)S(1)} %get-tuple-element.208, bf16[1024,8,128]{0,2,1:T(8,128)(2,1)S(1)} %bitcast.35), kind=kOutput, calls=%fused_computation.12 | convolution fusion | flops 402653184 | bytes 14024704 | tf_op jit(solution)/shard_map/while/body/eval_jaxpr/cond/branch_1_fun/thd,nhd->htn/dot_general | solution.py:55
  107.4 6.2 %fusion.64 = (f32[8,384]{1,0:T(8,128)S(1)}, f32[8,384,1024]{1,2,0:T(8,128)S(1)}) fusion(bf16[384,8,32]{0,2,1:T(8,128)(2,1)S(1)} %copy-done.3, bf16[3072,32]{0,1:T(8,128)(2,1)} %get-tuple-element.209, s32[]{:T(128)S(6)} %select_n.6, f32[8,1024,384]{2,1,0:T(8,128)} %fusion.13, pred[384,1024]{0,1:T(8,128)(4,1)S(1)} %broadcast_compare_fusion), kind=kOutput, calls=%fused_computation.98 | convolution fusion | flops 213906432 | bytes 25833476 | tf_op jit(solution)/shard_map/while/body/eval_jaxpr/cond/branch_1_fun/thr,nr->htn/dot_general | solution.py:56
  115.4 2.3 %fusion.9 = f32[8,384,64]{1,2,0:T(8,128)S(1)} fusion(f32[8,384,1024]{1,2,0:T(8,128)S(1)} %get-tuple-element.292, f32[8,384]{1,0:T(8,128)S(1)} %max.2, bf16[1024,8,128]{0,2,1:T(8,128)(2,1)S(1)} %bitcast.36, f32[8,384,64]{1,2,0:T(8,128)S(1)} %copy-done.1, f32[8,384]{1,0:T(8,128)S(1)} %get-tuple-element.290), kind=kOutput, calls=%fused_computation.10 | convolution fusion | flops 409337856 | bytes 15228928 | tf_op jit(solution)/shard_map/while/body/eval_jaxpr/cond/branch_1_fun/htn,nhd->htd/dot_general | solution.py:66
  118.6 20.7 %conditional.3 = ((f32[8,384]{1,0:T(8,128)S(1)}, f32[8,384]{1,0:T(8,128)}, f32[8,384,64]{1,2,0:T(8,128)})) conditional(s32[]{:T(128)} %convert_element_type.206, (f32[8,384]{1,0:T(8,128)S(1)}, f32[8,384]{1,0:T(8,128)}, f32[8,384,64]{1,2,0:T(8,128)}) %tuple.57, (s32[]{:T(128)}, s32[]{:T(128)}, bf16[3072,512]{1,0:T(8,128)(2,1)}, ...), branch_computations={%region_4.0_spmd, %region_5.7_spmd} | conditional | flops 2107383168 | bytes 79606488 | solution.py:168
  118.6 2.8 %convolution_convert_fusion = bf16[1024,1024]{0,1:T(8,128)(2,1)S(1)} fusion(bf16[512,1024]{1,0:T(8,128)(2,1)} %get-tuple-element.207, bf16[3072,512]{1,0:T(8,128)(2,1)} %get-tuple-element.206, s32[]{:T(128)S(6)} %select_n.6), kind=kOutput, calls=%fused_computation.9 | convolution fusion | flops 1074790400 | bytes 4194308 | tf_op jit(solution)/shard_map/while/body/eval_jaxpr/cond/branch_1_fun/dot_general | solution.py:147
  121.4 6.4 %fusion.13 = f32[8,1024,384]{2,1,0:T(8,128)} fusion(bf16[384,8,64]{0,2,1:T(8,128)(2,1)S(1)} %get-tuple-element.208, bf16[1024,8,128]{0,2,1:T(8,128)(2,1)S(1)} %bitcast.35), kind=kOutput, calls=%fused_computation.12 | convolution fusion | flops 402653184 | bytes 14024704 | tf_op jit(solution)/shard_map/while/body/eval_jaxpr/cond/branch_1_fun/thd,nhd->htn/dot_general | solution.py:55
  128.1 6.2 %fusion.64 = (f32[8,384]{1,0:T(8,128)S(1)}, f32[8,384,1024]{1,2,0:T(8,128)S(1)}) fusion(bf16[384,8,32]{0,2,1:T(8,128)(2,1)S(1)} %copy-done.3, bf16[3072,32]{0,1:T(8,128)(2,1)} %get-tuple-element.209, s32[]{:T(128)S(6)} %select_n.6, f32[8,1024,384]{2,1,0:T(8,128)} %fusion.13, pred[384,1024]{0,1:T(8,128)(4,1)S(1)} %broadcast_compare_fusion), kind=kOutput, calls=%fused_computation.98 | convolution fusion | flops 213906432 | bytes 25833476 | tf_op jit(solution)/shard_map/while/body/eval_jaxpr/cond/branch_1_fun/thr,nr->htn/dot_general | solution.py:56
  136.1 2.3 %fusion.9 = f32[8,384,64]{1,2,0:T(8,128)S(1)} fusion(f32[8,384,1024]{1,2,0:T(8,128)S(1)} %get-tuple-element.292, f32[8,384]{1,0:T(8,128)S(1)} %max.2, bf16[1024,8,128]{0,2,1:T(8,128)(2,1)S(1)} %bitcast.36, f32[8,384,64]{1,2,0:T(8,128)S(1)} %copy-done.1, f32[8,384]{1,0:T(8,128)S(1)} %get-tuple-element.290), kind=kOutput, calls=%fused_computation.10 | convolution fusion | flops 409337856 | bytes 15228928 | tf_op jit(solution)/shard_map/while/body/eval_jaxpr/cond/branch_1_fun/htn,nhd->htd/dot_general | solution.py:66
  139.2 20.7 %conditional.3 = ((f32[8,384]{1,0:T(8,128)S(1)}, f32[8,384]{1,0:T(8,128)}, f32[8,384,64]{1,2,0:T(8,128)})) conditional(s32[]{:T(128)} %convert_element_type.206, (f32[8,384]{1,0:T(8,128)S(1)}, f32[8,384]{1,0:T(8,128)}, f32[8,384,64]{1,2,0:T(8,128)}) %tuple.57, (s32[]{:T(128)}, s32[]{:T(128)}, bf16[3072,512]{1,0:T(8,128)(2,1)}, ...), branch_computations={%region_4.0_spmd, %region_5.7_spmd} | conditional | flops 2107383168 | bytes 79606488 | solution.py:168
  139.2 2.8 %convolution_convert_fusion = bf16[1024,1024]{0,1:T(8,128)(2,1)S(1)} fusion(bf16[512,1024]{1,0:T(8,128)(2,1)} %get-tuple-element.207, bf16[3072,512]{1,0:T(8,128)(2,1)} %get-tuple-element.206, s32[]{:T(128)S(6)} %select_n.6), kind=kOutput, calls=%fused_computation.9 | convolution fusion | flops 1074790400 | bytes 4194308 | tf_op jit(solution)/shard_map/while/body/eval_jaxpr/cond/branch_1_fun/dot_general | solution.py:147
  142.1 6.4 %fusion.13 = f32[8,1024,384]{2,1,0:T(8,128)} fusion(bf16[384,8,64]{0,2,1:T(8,128)(2,1)S(1)} %get-tuple-element.208, bf16[1024,8,128]{0,2,1:T(8,128)(2,1)S(1)} %bitcast.35), kind=kOutput, calls=%fused_computation.12 | convolution fusion | flops 402653184 | bytes 14024704 | tf_op jit(solution)/shard_map/while/body/eval_jaxpr/cond/branch_1_fun/thd,nhd->htn/dot_general | solution.py:55
  148.8 6.2 %fusion.64 = (f32[8,384]{1,0:T(8,128)S(1)}, f32[8,384,1024]{1,2,0:T(8,128)S(1)}) fusion(bf16[384,8,32]{0,2,1:T(8,128)(2,1)S(1)} %copy-done.3, bf16[3072,32]{0,1:T(8,128)(2,1)} %get-tuple-element.209, s32[]{:T(128)S(6)} %select_n.6, f32[8,1024,384]{2,1,0:T(8,128)} %fusion.13, pred[384,1024]{0,1:T(8,128)(4,1)S(1)} %broadcast_compare_fusion), kind=kOutput, calls=%fused_computation.98 | convolution fusion | flops 213906432 | bytes 25833476 | tf_op jit(solution)/shard_map/while/body/eval_jaxpr/cond/branch_1_fun/thr,nr->htn/dot_general | solution.py:56
  159.9 4.6 %fusion.46 = f32[384,2048,1]{1,0,2:T(8,128)} fusion(bf16[8,64,2048]{2,1,0:T(8,128)(2,1)} %bitcast.39, f32[8,384,64]{1,2,0:T(8,128)} %get-tuple-element.233, f32[8,384]{1,0:T(8,128)} %get-tuple-element.234), kind=kOutput, calls=%fused_computation.60 | convolution fusion | flops 805699584 | bytes 6041600 | tf_op jit(solution)/shard_map/htd,hdk->tk/dot_general | solution.py:175
  164.6 6.0 %fusion.22 = bf16[384,2048]{1,0:T(8,128)(2,1)} fusion(f32[384,2048,1]{1,0,2:T(8,128)} %fusion.46, bf16[256,2048]{1,0:T(8,128)(2,1)} %param.34, bf16[2048,256]{1,0:T(8,128)(2,1)} %param.22, bf16[384,2048]{1,0:T(8,128)(2,1)} %all-gather.3.cloned.1.call-done, f32[2048]{0:T(1024)S(1)} %copy-done.12, bf16[384,256]{1,0:T(8,128)(2,1)S(1)} %copy-done.10, ...), kind=kOutput, calls=%fused_computation.29 | convolution fusion | flops 811106304 | bytes 8599040 | tf_op jit(solution)/shard_map/dot_general | solution.py:178
  171.2 28.0 %reduce-scatter.2.cloned.1.call-done = bf16[384,512]{1,0:T(8,128)(2,1)} async-done(((bf16[384,2048]{1,0:T(8,128)(2,1)}), bf16[384,512]{1,0:T(8,128)(2,1)}) %reduce-scatter.2.cloned.1.call-update) | async-done | bytes 393232 | tf_op jit(solution)/shard_map/reduce_scatter | solution.py:181
  200.4 5.9 %psum.7 = f32[384]{0:T(512)S(1)} all-reduce(f32[384]{0:T(512)S(1)} %fusion.33), channel_id=1, replica_groups=mesh['sp'=8,'tp'=4] {'tp'}, use_global_device_ids=true, to_apply=%region_11.12 | all-reduce | flops 384 | bytes 3072 | tf_op jit(solution)/shard_map/psum | solution.py:184
  (128 shorter events, 27.2 us)
Async XLA Ops:
  7.2 30.0 %copy-start = (bf16[2048,768]{1,0:T(8,128)(2,1)S(1)}, bf16[2048,768]{1,0:T(8,128)(2,1)}, u32[]{:S(2)}) copy-start(bf16[2048,768]{1,0:T(8,128)(2,1)} %param.26) | copy-start | bytes 9437188
  7.2 23.4 %all-gather.3.cloned.1.call-start = ((), (), s32[]{:S(2)}) async-start(), calls=%async_computation.1 | async-start | bytes 1966080 | tf_op jit(solution)/shard_map/all_gather | solution.py:99
  7.9 88.4 %all-gather.5.cloned.1.call-start = ((), (), s32[]{:S(2)}) async-start(), calls=%async_computation.2 | async-start | bytes 3538944 | tf_op jit(solution)/shard_map/all_gather | solution.py:151
  32.4 13.3 %copy-start.13 = (f32[384]{0:T(512)}, f32[384]{0:T(512)S(1)}, u32[]{:S(2)}) copy-start(f32[384]{0:T(512)S(1)} %add_rsqrt_fusion.3) | copy-start | bytes 4612
  32.4 3.2 %copy-start.20 = (f32[512]{0:T(512)S(1)}, f32[512]{0:T(512)}, u32[]{:S(2)}) copy-start(f32[512]{0:T(512)} %param.31) | copy-start | bytes 6148
  32.4 4.2 %copy-start.15 = (bf16[3,256]{1,0:T(4,128)(2,1)S(1)}, bf16[3,256]{1,0:T(4,128)(2,1)}, u32[]{:S(2)}) copy-start(bf16[3,256]{1,0:T(4,128)(2,1)} %param.25) | copy-start | bytes 4612
  32.4 4.8 %copy-start.11 = (f32[2048]{0:T(1024)S(1)}, f32[2048]{0:T(1024)}, u32[]{:S(2)}) copy-start(f32[2048]{0:T(1024)} %param.21) | copy-start | bytes 24580
  36.5 162.7 %reduce-scatter.2.cloned.1.call-start = ((), (), s32[]{:S(2)}) async-start(), calls=%async_computation.3 | async-start | bytes 1966080 | tf_op jit(solution)/shard_map/reduce_scatter | solution.py:181
  37.2 3.0 %copy-start.5 = (bf16[768,768]{1,0:T(8,128)(2,1)S(1)}, bf16[768,768]{1,0:T(8,128)(2,1)}, u32[]{:S(2)}) copy-start(bf16[768,768]{1,0:T(8,128)(2,1)} %param.28) | copy-start | bytes 3538948
  37.2 3.0 %copy-start.19 = (f32[768]{0:T(1024)S(1)}, f32[768]{0:T(1024)}, u32[]{:S(2)}) copy-start(f32[768]{0:T(1024)} %param.27) | copy-start | bytes 9220
  43.1 2.5 %copy-start.24 = (bf16[2048,32]{0,1:T(8,128)(2,1)S(1)}, bf16[2048,32]{0,1:T(8,128)(2,1)}, u32[]{:S(2)}) copy-start(bf16[2048,32]{0,1:T(8,128)(2,1)} %param.30) | copy-start | bytes 393220
  43.7 30.3 %copy-start.9 = (bf16[384,256]{1,0:T(8,128)(2,1)}, bf16[384,256]{1,0:T(8,128)(2,1)S(1)}, u32[]{:S(2)}) copy-start(bf16[384,256]{1,0:T(8,128)(2,1)S(1)} %fusion.30) | copy-start | bytes 589828
  44.3 120.2 %collective-permute-start = (bf16[2,256]{1,0:T(2,128)(2,1)}, bf16[2,256]{1,0:T(2,128)(2,1)}, u32[]{:S(2)}, u32[]{:S(2)}) collective-permute-start(bf16[2,256]{1,0:T(2,128)(2,1)} %slice.61), channel_id=1, source_target_pairs={{0,4},{4,8},{8,12},{12,16},{16,20},{20,24},{24,28},{1,5},{5,9},{9,... | collective-permute-start | bytes 3080 | tf_op jit(solution)/shard_map/ppermute | solution.py:21
  100.7 6.7 %copy-start.3 = (bf16[384,8,32]{0,2,1:T(8,128)(2,1)S(1)}, bf16[384,8,32]{0,2,1:T(8,128)(2,1)}, u32[]{:S(2)}) copy-start(bf16[384,8,32]{0,2,1:T(8,128)(2,1)} %get-tuple-element.210) | copy-start | bytes 589828 | tf_op jit(solution)/shard_map/while/body/eval_jaxpr/cond
  121.4 6.7 %copy-start.3 = (bf16[384,8,32]{0,2,1:T(8,128)(2,1)S(1)}, bf16[384,8,32]{0,2,1:T(8,128)(2,1)}, u32[]{:S(2)}) copy-start(bf16[384,8,32]{0,2,1:T(8,128)(2,1)} %get-tuple-element.210) | copy-start | bytes 589828 | tf_op jit(solution)/shard_map/while/body/eval_jaxpr/cond
  142.1 6.7 %copy-start.3 = (bf16[384,8,32]{0,2,1:T(8,128)(2,1)S(1)}, bf16[384,8,32]{0,2,1:T(8,128)(2,1)}, u32[]{:S(2)}) copy-start(bf16[384,8,32]{0,2,1:T(8,128)(2,1)} %get-tuple-element.210) | copy-start | bytes 589828 | tf_op jit(solution)/shard_map/while/body/eval_jaxpr/cond
  159.9 4.6 %copy-start.10 = (bf16[384,256]{1,0:T(8,128)(2,1)S(1)}, bf16[384,256]{1,0:T(8,128)(2,1)}, u32[]{:S(2)}) copy-start(bf16[384,256]{1,0:T(8,128)(2,1)} %copy-done.9) | copy-start | bytes 589828
  159.9 4.6 %copy-start.12 = (f32[2048]{0:T(1024)S(1)}, f32[2048]{0:T(1024)}, u32[]{:S(2)}) copy-start(f32[2048]{0:T(1024)} %param.21) | copy-start | bytes 24580
  159.9 4.6 %copy-start.14 = (f32[384]{0:T(512)S(1)}, f32[384]{0:T(512)}, u32[]{:S(2)}) copy-start(f32[384]{0:T(512)} %copy-done.13) | copy-start | bytes 4612
  159.9 4.6 %copy-start.16 = (f32[1,256]{1,0:T(1,128)S(1)}, f32[1,256]{1,0:T(1,128)}, u32[]{:S(2)}) copy-start(f32[1,256]{1,0:T(1,128)} %get-tuple-element.301) | copy-start | bytes 3076
  159.9 4.6 %copy-start.17 = (f32[1,256]{1,0:T(1,128)S(1)}, f32[1,256]{1,0:T(1,128)}, u32[]{:S(2)}) copy-start(f32[1,256]{1,0:T(1,128)} %get-tuple-element.302) | copy-start | bytes 3076
  159.9 4.6 %copy-start.18 = (f32[1,256]{1,0:T(1,128)S(1)}, f32[1,256]{1,0:T(1,128)}, u32[]{:S(2)}) copy-start(f32[1,256]{1,0:T(1,128)} %get-tuple-element.303) | copy-start | bytes 3076
  164.5 6.0 %copy-start.8 = (f32[8,384]{1,0:T(8,128)S(1)}, f32[8,384]{1,0:T(8,128)}, u32[]{:S(2)}) copy-start(f32[8,384]{1,0:T(8,128)} %get-tuple-element.234) | copy-start | bytes 36868
  164.6 41.7 %copy-start.21 = (f32[512]{0:T(512)S(1)}, f32[512]{0:T(512)}, u32[]{:S(2)}) copy-start(f32[512]{0:T(512)} %param.35) | copy-start | bytes 6148
  (15 other events, 24.1 us)
Sparse Core Ops, SparseCore 0:
  9.5 20.9 all-gather.2
  36.6 59.6 all-gather.4
  170.7 28.4 reduce-scatter.1
where the time goes:
time: 217 us; the launch traced here: 215 us
  waiting for transfers between devices  72.9 us (34%)
  matrix products  72.4 us (33%)
  blocking collectives  33.4 us (15%)
  between operations  14 us (6%)
  other arithmetic  13.8 us (6%)
  local copies, waits for them, and re-layouts  6.41 us (3%)
    reduce_scatter x1, waiting for transfers between devices, body(): lax.psum_scatter(partial_value.astype(jnp.bfloat16), 'tp', scatter_dimens...  28 us
    all_gather x1, blocking collectives, body(): lax.all_gather(rope_key, 'sp', axis=0, tiled=True)  27.5 us
    all_gather x1, waiting for transfers between devices, body(): wide = lax.all_gather(tokens, 'tp', axis=1, tiled=True).astype(jnp.float32)  22.6 us
    all_gather x1, waiting for transfers between devices, body(): lax.all_gather(latent, 'sp', axis=0, tiled=True)  21.6 us
    dot_general x3, matrix products, attend(): jnp.einsum('thd,nhd->htn', query_plain, key_plain, preferred_element_type...  19.2 us
    dot_general x3, matrix products, attend(): jnp.einsum('thr,nr->htn', query_turned, key_turned, preferred_element_typ...  18.6 us
    dot_general x3, matrix products, expand_latent(): jnp.dot(block, kv_up_weight, preferred_element_type=jnp.float32)  8.51 us
    dot_general x5, matrix products, body(): jnp.dot(scaled, weight, preferred_element_type=jnp.float32)  7.87 us
  transfers between devices with their start and end apart: 4, of which 3 were waited for; matrix products, arithmetic and copies ran while one was open for 34% of the time, Pallas kernels for 0%

commit v1 on v0

v1 whole, which is shorter than its diff:
```python
import functools
import math

import jax
import jax.numpy as jnp
from jax import lax
from jax.experimental import pallas as pl
from jax.experimental.pallas import tpu as pltpu
from jax.sharding import PartitionSpec as P

NOPE = 64
ROPE = 32
VDIM = 64
TAPS = 3
LANES = 128

EPSILON = 1e-06
THETA = 500000.0
NEGATIVE = -1e30
MESH = pl.DeviceIdType.MESH
BF = jnp.bfloat16
F32 = jnp.float32


def remote(src, dst, send, recv, **where):
    return pltpu.make_async_remote_copy(
        src_ref=src, dst_ref=dst, send_sem=send, recv_sem=recv, device_id=where, device_id_type=MESH
    )


def dot(a, b):
    return jnp.dot(a, b, preferred_element_type=F32)


def greet_tp(tp, n):
    barrier = pltpu.get_barrier_semaphore()
    for step in range(1, n):
        pl.semaphore_signal(
            barrier, inc=1, device_id={"tp": lax.rem(tp + step, n)}, device_id_type=MESH
        )
    pl.semaphore_wait(barrier, n - 1)


def project_kernel(
    n, chunk,
    tok, pre, qg, kg, cos, sin, wo, wi, ws, wq, wk, wr,
    outer, driven, qn, kvb,
    buf, vo, vi, vs, vq, vk, vr, wsem, own_s, own_r, y_s, y_r, f_s, f_r,
):
    tp = lax.axis_index("tp")
    ny = n // 2
    y, core = tp // 2, lax.rem(tp, 2)
    partner = tp + 1 - 2 * core
    rows, width = tok.shape
    count = rows // chunk
    loads = [
        pltpu.make_async_copy(a, b, wsem.at[i])
        for i, (a, b) in enumerate(((wo, vo), (wi, vi), (ws, vs), (wq, vq), (wk, vk), (wr, vr)))
    ]
    greet_tp(tp, n)

    def part(r):
        return pl.ds(r * chunk, chunk)

    def y_copy(r, step):
        to = lax.rem(y + step, ny) * 2 + core
        return remote(
            tok.at[part(r)], buf.at[tp, part(r)], y_s.at[r, step], y_r.at[r, y], tp=to
        )

    def y_arrival(r, other):
        return remote(
            tok.at[part(r)], buf.at[other * 2 + core, part(r)], y_s.at[r, 0], y_r.at[r, other],
            tp=partner,
        )

    def own_copy(r):
        return remote(tok.at[part(r)], buf.at[tp, part(r)], own_s.at[r], own_r.at[r], tp=partner)

    def forward(r, other):
        here = buf.at[other * 2 + core, part(r)]
        return remote(here, here, f_s.at[r, other], f_r.at[r, other], tp=partner)

    for r in range(count):
        for step in range(1, ny):
            y_copy(r, step).start()
    for r in range(count):
        own_copy(r).start()
    for load in loads:
        load.start()
    buf[tp] = tok[...]
    for load in loads:
        load.wait()

    def compute(r, carry):
        for step in range(1, ny):
            other = lax.rem(y + ny - step, ny)
            y_arrival(r, other).wait_recv()
            forward(r, other).start()
        own_copy(r).wait_recv()
        for step in range(1, ny):
            other = lax.rem(y + ny - step, ny)
            forward(r, other).wait_recv()
        here = pl.ds(pl.multiple_of(r * chunk, chunk), chunk)
        total = n * width
        wide = jnp.concatenate([buf[s, here] for s in range(n)], axis=1).astype(F32)
        factor = lax.rsqrt(jnp.sum(wide * wide, axis=1, keepdims=True) / total + EPSILON)
        scaled = (wide * pre[...]).astype(BF)
        kv = dot(scaled, vk[...]) * factor
        kv = kv * lax.rsqrt(jnp.mean(kv * kv, axis=1, keepdims=True) + EPSILON) * kg[...]
        rank = kv.shape[1]
        kvb[here, :rank] = kv.astype(BF)
        turn = dot(scaled, vr[...]) * factor
        swapped = jnp.concatenate([turn[:, ROPE // 2 :], turn[:, : ROPE // 2]], axis=1)
        turn = turn * cos[here] + swapped * sin[here]
        kvb[here, rank:] = jnp.concatenate(
            [turn, jnp.zeros((chunk, LANES - ROPE), F32)], axis=1
        ).astype(BF)
        q = dot(scaled, vq[...]) * factor
        q = q * lax.rsqrt(jnp.mean(q * q, axis=1, keepdims=True) + EPSILON) * qg[...]
        qn[here] = q.astype(BF)
        outer[here] = (dot(scaled, vo[...]) * factor).astype(BF)
        inner = (dot(scaled, vi[...]) * factor).astype(BF).astype(F32)
        source = (dot(scaled, vs[...]) * factor).astype(BF).astype(F32)
        driven[here] = (inner * source).astype(BF)
        return carry

    lax.fori_loop(0, count, compute, 0)
    for r in range(count):
        own_copy(r).wait_send()
        for step in range(1, ny):
            y_copy(r, step).wait_send()
            forward(r, lax.rem(y + step, ny)).wait_send()


def attend_kernel(
    nz, nx, ntp, heads,
    kvb, qt, up,
    att, logs,
    buf, kv, acc, top, low, z_s, x_s, d_s, i_r, d_r,
):
    sp, tp = lax.axis_index("sp"), lax.axis_index("tp")
    z, x = sp // nx, lax.rem(sp, nx)
    core = lax.rem(tp, 2)
    partner = tp + 1 - 2 * core
    rows = kvb.shape[0]
    half = rows // 2
    rank = up.shape[0]
    scale = (NOPE + ROPE) ** (-0.5)
    factor = scale * math.log2(math.e)
    mine = pl.ds(pl.multiple_of(core * half, half), half)

    barrier = pltpu.get_barrier_semaphore()

    def greet(**where):
        pl.semaphore_signal(barrier, inc=1, device_id=where, device_id_type=MESH)

    greet(tp=partner)
    for step in range(1, nx):
        greet(sp=z * nx + lax.rem(x + step, nx))

    @pl.when(z > 0)
    def _():
        greet(sp=sp - nx)

    @pl.when(z < nz - 1)
    def _():
        greet(sp=sp + nx)

    inside = jnp.where(z > 0, 1, 0) + jnp.where(z < nz - 1, 1, 0)
    pl.semaphore_wait(barrier, nx + inside)

    def up_copy(k):
        src = sp - k * nx
        return remote(buf.at[src, mine], buf.at[src, mine], z_s.at[k], i_r.at[src], sp=sp + nx)

    def side_copy(k, step):
        src = sp - k * nx
        to = z * nx + lax.rem(x + step, nx)
        return remote(buf.at[src, mine], buf.at[src, mine], x_s.at[k, step], i_r.at[src], sp=to)

    def own_up():
        return remote(kvb.at[mine], buf.at[sp, mine], z_s.at[0], i_r.at[sp], sp=sp + nx)

    def own_side(step):
        to = z * nx + lax.rem(x + step, nx)
        return remote(kvb.at[mine], buf.at[sp, mine], x_s.at[0, step], i_r.at[sp], sp=to)

    def arrival(src):
        return remote(kvb.at[mine], buf.at[src, mine], z_s.at[0], i_r.at[src], tp=partner)

    def share(src):
        return remote(buf.at[src, mine], buf.at[src, mine], d_s.at[src], d_r.at[src], tp=partner)

    @pl.when(z < nz - 1)
    def _():
        own_up().start()

    for step in range(1, nx):
        @pl.when(x + step < nx)
        def _(step=step):
            own_side(step).start()

    def compute(block, first):
        lat = block[:, :rank]
        turn = block[:, rank:]
        for h in range(heads):
            kv[h] = dot(lat, up[:, h * LANES : (h + 1) * LANES]).astype(BF)

        def one(h):
            keyval = kv[h]
            scores = dot(jnp.concatenate([keyval, turn], axis=1), qt[h])
            if first:
                key = lax.broadcasted_iota(jnp.int32, scores.shape, 0)
                query = lax.broadcasted_iota(jnp.int32, scores.shape, 1)
                scores = jnp.where(key <= query, scores, NEGATIVE)
            peak = jnp.max(scores, axis=0, keepdims=True) * factor
            if not first:
                before = top[h]
                peak = jnp.maximum(before, peak)
            weights = jnp.exp2(scores * factor - peak)
            total = jnp.sum(weights, axis=0, keepdims=True)
            values = lax.dot_general(
                keyval, weights.astype(BF), (((0,), (0,)), ((), ())), preferred_element_type=F32
            )
            if not first:
                shrink = jnp.exp2(before - peak)
                total = total + low[h] * shrink
                values = values + acc[h] * shrink
            top[h] = peak
            low[h] = total
            acc[h] = values

        def pair(i, carry):
            one(2 * i)
            one(2 * i + 1)
            return carry

        lax.fori_loop(0, heads // 2, pair, 0)

    compute(kvb[...], True)

    def receive_side(src):
        arrival(src).wait_recv()
        share(src).start()
        share(src).wait_recv()
        compute(buf[src], False)

    def side_loop(k, low_step):
        def run(step, carry):
            receive_side((z - k) * nx + lax.rem(x + step, nx))
            return carry

        lax.fori_loop(low_step, nx, run, 0)

    side_loop(0, nx - x)

    def level(k, carry):
        src = sp - k * nx
        arrival(src).wait_recv()

        @pl.when(z < nz - 1)
        def _():
            up_copy(k).start()

        for step in range(1, nx):
            side_copy(k, step).start()
        share(src).start()
        share(src).wait_recv()
        compute(buf[src], False)
        side_loop(k, 1)
        return carry

    lax.fori_loop(1, z + 1, level, 0)

    for i in range(heads // 2):
        both = jnp.concatenate(
            [acc[2 * i, NOPE:] / low[2 * i], acc[2 * i + 1, NOPE:] / low[2 * i + 1]], axis=0
        )
        att[:, i * LANES : (i + 1) * LANES] = both.T.astype(BF)
    for h in range(heads):
        logs[h : h + 1, :] = top[h] * math.log(2.0) + jnp.log(low[h])

    @pl.when(z < nz - 1)
    def _():
        own_up().wait_send()

    for step in range(1, nx):
        @pl.when(x + step < nx)
        def _(step=step):
            own_side(step).wait_send()

    def side_sent(k, low_step):
        def run(step, carry):
            share((z - k) * nx + lax.rem(x + step, nx)).wait_send()
            return carry

        lax.fori_loop(low_step, nx, run, 0)

    side_sent(0, nx - x)

    def sent(k, carry):
        @pl.when(z < nz - 1)
        def _():
            up_copy(k).wait_send()

        for step in range(1, nx):
            side_copy(k, step).wait_send()
        share(sp - k * nx).wait_send()
        side_sent(k, 1)
        return carry

    lax.fori_loop(1, z + 1, sent, 0)


def finish_kernel(
    n, chunk,
    att, conv, wa, wc, gain,
    out,
    away, mine, pin, ysend, yin, peer, pown, total, sq, sqin,
    a_s, a_r, y_s, y_r, p_s, p_r, q_s, q_r,
):
    tp = lax.axis_index("tp")
    ny = n // 2
    y, core = tp // 2, lax.rem(tp, 2)
    partner = tp + 1 - 2 * core
    rows, width = out.shape
    count = rows // chunk
    greet_tp(tp, n)

    def part(r):
        return pl.ds(r * chunk, chunk)

    def product(r, dest):
        columns = pl.ds(pl.multiple_of(dest * width, width), width)
        return (dot(att[part(r)], wa[:, columns]) + dot(conv[part(r)], wc[:, columns])).astype(BF)

    def to_partner(r, step):
        return remote(
            away.at[step, part(r)], pin.at[step, part(r)], a_s.at[r, step], a_r.at[r, step], tp=partner
        )

    def across(r, step):
        to = lax.rem(y + step, ny) * 2 + core
        return remote(
            ysend.at[step, part(r)], yin.at[step, part(r)], y_s.at[r, step], y_r.at[r, step], tp=to
        )

    def home(r):
        return remote(peer.at[part(r)], pown.at[part(r)], p_s.at[r], p_r.at[r], tp=partner)

    def squares(step):
        return remote(
            sq, sqin.at[step], q_s.at[step], q_r.at[step], tp=lax.rem(tp + step, n)
        )

    for r in range(count):
        for step in range(1, ny):
            dest = lax.rem(y + step, ny) * 2
            away[step, part(r)] = product(r, dest + 1 - core)
            to_partner(r, step).start()
            mine[step, part(r)] = product(r, dest + core)
    for r in range(count):
        for step in range(1, ny):
            to_partner(r, step).wait_recv()
            ysend[step, part(r)] = (
                mine[step, part(r)].astype(F32) + pin[step, part(r)].astype(F32)
            ).astype(BF)
            across(r, step).start()
    for r in range(count):
        peer[part(r)] = product(r, partner)
        home(r).start()
        total[part(r)] = product(r, tp).astype(F32)
    for r in range(count):
        home(r).wait_recv()
        total[part(r)] += pown[part(r)].astype(F32)
    for r in range(count):
        for step in range(1, ny):
            across(r, step).wait_recv()
            total[part(r)] += yin[step, part(r)].astype(F32)
        value = total[part(r)]
        sums = jnp.sum(value * value, axis=1, keepdims=True)
        sq[:, part(r)] = jnp.broadcast_to(sums, (chunk, LANES)).T[:8]
    for step in range(1, n):
        squares(step).start()
    whole = sq[...]
    for step in range(1, n):
        squares(step).wait_recv()
        whole = whole + sqin[step]
    scale = lax.rsqrt(whole / (n * width) + EPSILON)
    for r in range(count):
        column = jnp.broadcast_to(
            scale[:1, r * chunk : (r + 1) * chunk], (LANES, chunk)
        ).T[:, :1]
        out[part(r)] = (total[part(r)] * column * gain[...]).astype(BF)
    for r in range(count):
        home(r).wait_send()
        for step in range(1, ny):
            to_partner(r, step).wait_send()
            across(r, step).wait_send()
    for step in range(1, n):
        squares(step).wait_send()


def vmem(count):
    return [pl.BlockSpec(memory_space=pltpu.VMEM)] * count


def params(collective):
    return pltpu.CompilerParams(
        collective_id=collective, has_side_effects=True, vmem_limit_bytes=56 * 1024 * 1024
    )


DMA = pltpu.SemaphoreType.DMA


def body(
    nsp, ntp,
    tokens, pre_gain, outer_gate_weight, inner_gate_weight, source_weight, conv_taps,
    q_down_weight, q_norm_gain, q_up_weight, kv_down_weight, rope_key_weight, kv_norm_gain,
    kv_up_weight, attn_out_weight, conv_out_weight, post_gain,
):
    rows, width = tokens.shape
    ny = ntp // 2
    nx = ny if nsp % ny == 0 else 1
    nz = nsp // nx
    chunk = LANES
    count = rows // chunk
    q_rank, kv_rank = q_down_weight.shape[1], kv_down_weight.shape[1]
    channels = outer_gate_weight.shape[1]
    heads = q_up_weight.shape[1] // (NOPE + ROPE)
    struct = jax.ShapeDtypeStruct
    sp = lax.axis_index("sp")

    pos = (sp * rows + jnp.arange(rows, dtype=jnp.int32)).astype(F32)
    freqs = THETA ** (-jnp.arange(0, ROPE, 2, dtype=F32) / ROPE)
    angles = pos[:, None] * freqs[None, :]
    cosine, sine = jnp.cos(angles), jnp.sin(angles)
    cos_full = jnp.concatenate([cosine, cosine], axis=1)
    sin_full = jnp.concatenate([-sine, sine], axis=1)

    weights = (
        outer_gate_weight, inner_gate_weight, source_weight,
        q_down_weight, kv_down_weight, rope_key_weight,
    )
    outer, driven, q_normed, kvb = pl.pallas_call(
        functools.partial(project_kernel, ntp, chunk),
        out_shape=[
            struct((rows, channels), BF), struct((rows, channels), BF),
            struct((rows, q_rank), BF), struct((rows, kv_rank + LANES), BF),
        ],
        in_specs=vmem(6) + [pl.BlockSpec(memory_space=pl.ANY)] * 6,
        out_specs=vmem(4),
        scratch_shapes=[pltpu.VMEM((ntp, rows, width), BF)]
        + [pltpu.VMEM(w.shape, BF) for w in weights]
        + [
            DMA((6,)), DMA((count,)), DMA((count,)), DMA((count, ny)), DMA((count, ny)),
            DMA((count, ny)), DMA((count, ny)),
        ],
        compiler_params=params(0),
        name="project",
    )(
        tokens, pre_gain[None], q_norm_gain[None], kv_norm_gain[None], cos_full, sin_full, *weights
    )

    query = lax.dot_general(
        q_up_weight, q_normed, (((0,), (1,)), ((), ())), preferred_element_type=F32
    ).reshape(heads, NOPE + ROPE, rows)
    first, second = query[:, NOPE : NOPE + ROPE // 2], query[:, NOPE + ROPE // 2 :]
    ct, st = cosine.T[None], sine.T[None]
    qt = jnp.concatenate(
        [
            query[:, :NOPE], jnp.zeros((heads, VDIM, rows), F32),
            first * ct - second * st, second * ct + first * st,
            jnp.zeros((heads, LANES - ROPE, rows), F32),
        ],
        axis=1,
    ).astype(BF)

    attended, log_total = pl.pallas_call(
        functools.partial(attend_kernel, nz, nx, ntp, heads),
        out_shape=[struct((rows, heads * VDIM), BF), struct((heads, rows), F32)],
        in_specs=vmem(3),
        out_specs=vmem(2),
        scratch_shapes=[
            pltpu.VMEM((nsp, rows, kv_rank + LANES), BF),
            pltpu.VMEM((heads, rows, LANES), BF),
            pltpu.VMEM((heads, LANES, rows), F32),
            pltpu.VMEM((heads, 1, rows), F32),
            pltpu.VMEM((heads, 1, rows), F32),
            DMA((nz,)), DMA((nz, nx)), DMA((nsp,)), DMA((nsp,)), DMA((nsp,)),
        ],
        compiler_params=params(1),
        name="attend",
    )(kvb, qt, kv_up_weight)

    prior = lax.ppermute(driven[rows - (TAPS - 1) :], "sp", [(i, i + 1) for i in range(nsp - 1)])
    extended = jnp.concatenate([prior, driven], axis=0)
    convolved = jnp.zeros(driven.shape, F32)
    for index in range(TAPS):
        convolved = convolved + conv_taps[index].astype(F32) * extended[
            index : index + rows
        ].astype(F32)
    conv_branch = (outer.astype(F32) * convolved).astype(BF)

    block = (ny, rows, width)
    mixed = pl.pallas_call(
        functools.partial(finish_kernel, ntp, chunk),
        out_shape=struct((rows, width), BF),
        in_specs=vmem(5),
        out_specs=pl.BlockSpec(memory_space=pltpu.VMEM),
        scratch_shapes=[pltpu.VMEM(block, BF)] * 5
        + [
            pltpu.VMEM((rows, width), BF), pltpu.VMEM((rows, width), BF),
            pltpu.VMEM((rows, width), F32),
            pltpu.VMEM((8, rows), F32), pltpu.VMEM((ntp, 8, rows), F32),
            DMA((count, ny)), DMA((count, ny)), DMA((count, ny)), DMA((count, ny)),
            DMA((count,)), DMA((count,)), DMA((ntp,)), DMA((ntp,)),
        ],
        compiler_params=params(2),
        name="finish",
    )(attended, conv_branch, attn_out_weight, conv_out_weight, post_gain[None])
    return mixed, log_total


def solution(mesh):
    placed = (
        P("sp", "tp"), P(), P(None, "tp"), P(None, "tp"), P(None, "tp"), P(None, "tp"), P(), P(),
        P(None, "tp"), P(), P(), P(), P(None, "tp"), P("tp", None), P("tp", None), P("tp"),
    )
    return jax.shard_map(
        functools.partial(body, mesh.shape["sp"], mesh.shape["tp"]),
        mesh=mesh,
        in_specs=placed,
        out_specs=(P("sp", "tp"), P("tp", "sp")),
        check_vma=False,
    )
```

time: 217 us -> 114 us (0.53)
  Pallas kernels: 0 us -> 95.8 us
  waiting for transfers between devices: 72.9 us -> 0.01 us
  matrix products: 72.4 us -> 1.69 us
  blocking collectives: 33.4 us -> 0 us
  between operations: 14 us -> 0.83 us
  other arithmetic: 13.8 us -> 2.66 us
  local copies, waits for them, and re-layouts: 6.41 us -> 10.2 us
    pallas_call x0 -> x3, Pallas kernels: none -> 95.8 us  [the longest x1 59.3 us: body(): pl.pallas_call(functools.partial(attend_kernel, nz, nx, ntp, heads), out_...]
    dot_general x20 -> x1, matrix products: 72.4 us -> 1.69 us  [body(): lax.dot_general(q_up_weight, q_normed, (((0,), (1,)), ((), ())), preferre...]
    all_gather x2 -> x0, waiting for transfers between devices: 44.2 us -> none  [the longest x1 22.6 us: body(): wide = lax.all_gather(tokens, 'tp', axis=1, tiled=True).astype(jnp.float32)]
    reduce_scatter x1 -> x0, waiting for transfers between devices: 28 us -> none  [body(): lax.psum_scatter(partial_value.astype(jnp.bfloat16), 'tp', scatter_dimens...]
    all_gather x1 -> x0, blocking collectives: 27.5 us -> none  [body(): lax.all_gather(rope_key, 'sp', axis=0, tiled=True)]
    reduce_sum x5 -> x0, other arithmetic: 7.88 us -> none  [the longest x3 4.94 us: attend(): totals = totals * shrink + jnp.sum(weights, axis=-1)]
    psum x1 -> x0, blocking collectives: 5.87 us -> none  [body(): row_squares = lax.psum(jnp.sum(summed * summed, axis=1), 'tp')]
    unnamed x40 -> x21, local copies, waits for them, and re-layouts: 1.46 us -> 5.56 us
  transfers between devices with their start and end apart: 4 -> 1, of which waited for: 3 -> 0; matrix products, arithmetic and copies ran while one was open for 34% -> 3% of each run, Pallas kernels for 0% -> 53%
where the time goes in v1:
time: 114 us; the launch traced here: 113 us
  Pallas kernels  95.8 us (84%)
  local copies, waits for them, and re-layouts  10.2 us (9%)
  other arithmetic  2.66 us (2%)
  matrix products  1.69 us (1%)
  starting transfers between devices  1.28 us (1%)
    pallas_call x1, Pallas kernels, body(): pl.pallas_call(functools.partial(attend_kernel, nz, nx, ntp, heads), out_...  59.3 us
    pallas_call x1, Pallas kernels, body(): pl.pallas_call(functools.partial(finish_kernel, ntp, chunk), out_shape=st...  19.5 us
    pallas_call x1, Pallas kernels, body(): pl.pallas_call(functools.partial(project_kernel, ntp, chunk), out_shape=[...  17 us
    unnamed x21, local copies, waits for them, and re-layouts  5.56 us
  transfers between devices with their start and end apart: 1, of which 0 were waited for; matrix products, arithmetic and copies ran while one was open for 3% of the time, Pallas kernels for 53%

profile of v1, /device:TPU:27, one launch (start us, length us, event | category | flops | bytes accessed | tf_op | source)
XLA Modules:
  0.0 112.5 jit_solution(13393789208748184904)
XLA Ops:
  0.6 0.0 copy-start
  0.7 1.4 %broadcast_in_dim.26.qg = f32[1,768]{1,0:T(1,128)} reshape(f32[768]{0:T(1024)} %param.23) | data formatting | bytes 6144 | tf_op jit(solution)/shard_map/broadcast_in_dim | solution.py:464
  2.0 0.2 fusion.4
  2.2 0.8 copy.20.cos
  3.0 0.8 copy.21.sin
  3.8 1.9 %copy.22.wr = bf16[2048,32]{1,0:T(8,128)(2,1)} copy(bf16[2048,32]{0,1:T(8,128)(2,1)} %param.26) | data formatting | bytes 262144 | tf_op args[10]
  5.8 17.0 %project.1 = (bf16[384,256]{1,0:T(8,128)(2,1)}, bf16[384,256]{1,0:T(8,128)(2,1)}, bf16[384,768]{1,0:T(8,128)(2,1)}, bf16[384,640]{1,0:T(8,128)(2,1)}) custom-call(bf16[384,512]{1,0:T(8,128)(2,1)} %tok.1, f32[1,2048]{1,0:T(1,128)} %bitcast.14, f32[1,768]{1,0:T(1,128)} %broadcast_in_dim.26.qg, f32[1,512]{1,0:T(1,128)} %bitcast.19, f32[384,32]{1,0:T(8,128)} %copy.20.cos, ...), custom_call_target="tpu_custom_call" | custom-call | tf_op jit(solution)/shard_map/project/pallas_call | solution.py:447
  22.8 1.2 %slice.32 = bf16[2,256]{1,0:T(2,128)(2,1)} slice(bf16[384,256]{1,0:T(8,128)(2,1)} %get-tuple-element.12), slice={[382:384], [0:256]} | slice | bytes 2048 | tf_op jit(solution)/shard_map/slice | solution.py:498
  24.0 1.3 %collective-permute-start = (bf16[2,256]{1,0:T(2,128)(2,1)}, bf16[2,256]{1,0:T(2,128)(2,1)S(1)}, u32[]{:S(2)}, u32[]{:S(2)}) collective-permute-start(bf16[2,256]{1,0:T(2,128)(2,1)} %slice.32), channel_id=1, source_target_pairs={{0,4},{4,8},{8,12},{12,16},{16,20},{20,24},{24,28},{1,5},{5,9},{9,... | collective-permute-start | bytes 3080 | tf_op jit(solution)/shard_map/ppermute | solution.py:498
  25.3 0.8 multiply_cosine_fusion
  26.1 1.7 %convolution_bitcast_fusion = f32[768,384]{0,1:T(8,128)S(1)} fusion(bf16[384,768]{1,0:T(8,128)(2,1)} %get-tuple-element.9, bf16[768,768]{1,0:T(8,128)(2,1)S(1)} %copy-done), kind=kOutput, calls=%fused_computation | convolution fusion | flops 452984832 | bytes 2949120 | tf_op jit(solution)/shard_map/dot_general | solution.py:467
  27.8 0.4 copy.23
  28.2 0.0 copy-start.2
  28.3 0.1 broadcast_dynamic-update-slice_fusion.1
  28.3 0.8 fusion.2
  29.2 0.1 broadcast_dynamic-update-slice_fusion.qt
  29.3 1.1 %copy-done.1 = bf16[8,256,384]{2,1,0:T(8,128)(2,1)} copy-done((bf16[8,256,384]{2,1,0:T(8,128)(2,1)}, bf16[8,256,384]{2,1,0:T(8,128)(2,1)S(1)}, u32[]{:S(2)}) %copy-start.1) | copy-done | bytes 1572888
  30.5 59.3 %attend.1 = (bf16[384,512]{1,0:T(8,128)(2,1)}, f32[8,384]{1,0:T(8,128)}) custom-call(bf16[384,640]{1,0:T(8,128)(2,1)} %get-tuple-element.8.kvb, bf16[8,256,384]{2,1,0:T(8,128)(2,1)} %copy-done.1, bf16[512,1024]{1,0:T(8,128)(2,1)} %up.1), custom_call_target="tpu_custom_call" | custom-call | tf_op jit(solution)/shard_map/attend/pallas_call | solution.py:481
  89.8 0.0 collective-permute-done
  89.8 0.0 copy-done.4
  89.8 0.8 multiply_convert_fusion.conv
  90.6 19.5 %finish.1 = bf16[384,512]{1,0:T(8,128)(2,1)} custom-call(bf16[384,512]{1,0:T(8,128)(2,1)} %get-tuple-element.10.att, bf16[384,256]{1,0:T(8,128)(2,1)} %multiply_convert_fusion.conv, bf16[512,2048]{1,0:T(8,128)(2,1)} %wa.1, bf16[256,2048]{1,0:T(8,128)(2,1)} %wc.1, f32[1,512]{1,0:T(1,128)} %bitcast.18), custom_call_target="tpu_custom_call" | custom-call | tf_op jit(solution)/shard_map/finish/pallas_call | solution.py:508
  110.2 1.8 %copy.30 = bf16[384,512]{1,0:T(8,128)(2,1)} copy(bf16[384,512]{1,0:T(8,128)(2,1)} %finish.1) | data formatting | bytes 786432
  111.9 0.6 copy.31
  (18 shorter events, 0.1 us)
Async XLA Ops:
  0.6 25.5 %copy-start = (bf16[768,768]{1,0:T(8,128)(2,1)S(1)}, bf16[768,768]{1,0:T(8,128)(2,1)}, u32[]{:S(2)}) copy-start(bf16[768,768]{1,0:T(8,128)(2,1)} %param.24) | copy-start | bytes 3538948
  5.8 20.3 %copy-start.7 = (bf16[3,256]{1,0:T(4,128)(2,1)S(1)}, bf16[3,256]{1,0:T(4,128)(2,1)}, u32[]{:S(2)}) copy-start(bf16[3,256]{1,0:T(4,128)(2,1)} %param.21) | copy-start | bytes 4612
  24.0 65.7 %collective-permute-start = (bf16[2,256]{1,0:T(2,128)(2,1)}, bf16[2,256]{1,0:T(2,128)(2,1)S(1)}, u32[]{:S(2)}, u32[]{:S(2)}) collective-permute-start(bf16[2,256]{1,0:T(2,128)(2,1)} %slice.32), channel_id=1, source_target_pairs={{0,4},{4,8},{8,12},{12,16},{16,20},{20,24},{24,28},{1,5},{5,9},{9,... | collective-permute-start | bytes 3080 | tf_op jit(solution)/shard_map/ppermute | solution.py:498
  28.2 0.9 copy-start.2
  28.2 0.9 copy-start.3
  29.3 1.2 %copy-start.1 = (bf16[8,256,384]{2,1,0:T(8,128)(2,1)}, bf16[8,256,384]{2,1,0:T(8,128)(2,1)S(1)}, u32[]{:S(2)}) copy-start(bf16[8,256,384]{2,1,0:T(8,128)(2,1)S(1)} %broadcast_dynamic-update-slice_fusion.qt) | copy-start | bytes 4718596
  29.3 60.5 %copy-start.4 = (bf16[384,256]{1,0:T(8,128)(2,1)S(1)}, bf16[384,256]{1,0:T(8,128)(2,1)}, u32[]{:S(2)}) copy-start(bf16[384,256]{1,0:T(8,128)(2,1)} %get-tuple-element.12) | copy-start | bytes 589828
  29.3 60.5 %copy-start.5 = (bf16[384,256]{1,0:T(8,128)(2,1)S(1)}, bf16[384,256]{1,0:T(8,128)(2,1)}, u32[]{:S(2)}) copy-start(bf16[384,256]{1,0:T(8,128)(2,1)} %get-tuple-element.11) | copy-start | bytes 589828
  90.6 21.3 %copy-start.6 = (f32[8,384]{1,0:T(8,128)S(1)}, f32[8,384]{1,0:T(8,128)}, u32[]{:S(2)}) copy-start(f32[8,384]{1,0:T(8,128)} %get-tuple-element.27) | copy-start | bytes 36868

commit v2 on v1

--- a/solution.py
+++ b/solution.py
@@ -110,9 +110,11 @@
         kv = kv * lax.rsqrt(jnp.mean(kv * kv, axis=1, keepdims=True) + EPSILON) * kg[...]
         rank = kv.shape[1]
         kvb[here, :rank] = kv.astype(BF)
-        turn = dot(scaled, vr[...]) * factor
+        turn = factor * lax.dot_general(
+            scaled, vr[...], (((1,), (1,)), ((), ())), preferred_element_type=F32
+        )
         swapped = jnp.concatenate([turn[:, ROPE // 2 :], turn[:, : ROPE // 2]], axis=1)
-        turn = turn * cos[here] + swapped * sin[here]
+        turn = turn * cos[:, here].T + swapped * sin[:, here].T
         kvb[here, rank:] = jnp.concatenate(
             [turn, jnp.zeros((chunk, LANES - ROPE), F32)], axis=1
         ).astype(BF)
@@ -204,8 +206,10 @@
     def compute(block, first):
         lat = block[:, :rank]
         turn = block[:, rank:]
-        for h in range(heads):
-            kv[h] = dot(lat, up[:, h * LANES : (h + 1) * LANES]).astype(BF)
+        for h in range(0, heads, 2):
+            both = dot(lat, up[:, h * LANES : (h + 2) * LANES]).astype(BF)
+            kv[h] = both[:, :LANES]
+            kv[h + 1] = both[:, LANES:]
 
         def one(h):
             keyval = kv[h]
@@ -240,38 +244,49 @@
 
     compute(kvb[...], True)
 
-    def receive_side(src):
-        arrival(src).wait_recv()
-        share(src).start()
+    def side_source(k, step):
+        return (z - k) * nx + lax.rem(x + step, nx)
+
+    def side_share(k, low_step):
+        def run(step, carry):
+            src = side_source(k, step)
+            arrival(src).wait_recv()
+            share(src).start()
+            return carry
+
+        lax.fori_loop(low_step, nx, run, 0)
+
+    def shared_compute(src):
         share(src).wait_recv()
         compute(buf[src], False)
 
-    def side_loop(k, low_step):
-        def run(step, carry):
-            receive_side((z - k) * nx + lax.rem(x + step, nx))
-            return carry
-
-        lax.fori_loop(low_step, nx, run, 0)
-
-    side_loop(0, nx - x)
-
     def level(k, carry):
         src = sp - k * nx
-        arrival(src).wait_recv()
-
-        @pl.when(z < nz - 1)
+        fresh = k <= z
+
+        @pl.when(fresh)
         def _():
-            up_copy(k).start()
-
-        for step in range(1, nx):
-            side_copy(k, step).start()
-        share(src).start()
-        share(src).wait_recv()
-        compute(buf[src], False)
-        side_loop(k, 1)
+            arrival(src).wait_recv()
+            share(src).start()
+
+            @pl.when(z < nz - 1)
+            def _():
+                up_copy(k).start()
+
+            for step in range(1, nx):
+                side_copy(k, step).start()
+
+        low_step = jnp.where(k == 1, nx - x, 1)
+        side_share(k - 1, low_step)
+
+        def run(step, carry):
+            shared_compute(jnp.where(step == 0, src, side_source(k - 1, step + low_step - 1)))
+            return carry
+
+        lax.fori_loop(jnp.where(fresh, 0, 1), nx - low_step + 1, run, 0)
         return carry
 
-    lax.fori_loop(1, z + 1, level, 0)
+    lax.fori_loop(1, z + 2, level, 0)
 
     for i in range(heads // 2):
         both = jnp.concatenate(
@@ -435,14 +450,14 @@
 
     pos = (sp * rows + jnp.arange(rows, dtype=jnp.int32)).astype(F32)
     freqs = THETA ** (-jnp.arange(0, ROPE, 2, dtype=F32) / ROPE)
-    angles = pos[:, None] * freqs[None, :]
+    angles = freqs[:, None] * pos[None, :]
     cosine, sine = jnp.cos(angles), jnp.sin(angles)
-    cos_full = jnp.concatenate([cosine, cosine], axis=1)
-    sin_full = jnp.concatenate([-sine, sine], axis=1)
+    cos_full = jnp.concatenate([cosine, cosine], axis=0)
+    sin_full = jnp.concatenate([-sine, sine], axis=0)
 
     weights = (
         outer_gate_weight, inner_gate_weight, source_weight,
-        q_down_weight, kv_down_weight, rope_key_weight,
+        q_down_weight, kv_down_weight, rope_key_weight.T,
     )
     outer, driven, q_normed, kvb = pl.pallas_call(
         functools.partial(project_kernel, ntp, chunk),
@@ -468,7 +483,7 @@
         q_up_weight, q_normed, (((0,), (1,)), ((), ())), preferred_element_type=F32
     ).reshape(heads, NOPE + ROPE, rows)
     first, second = query[:, NOPE : NOPE + ROPE // 2], query[:, NOPE + ROPE // 2 :]
-    ct, st = cosine.T[None], sine.T[None]
+    ct, st = cosine[None], sine[None]
     qt = jnp.concatenate(
         [
             query[:, :NOPE], jnp.zeros((heads, VDIM, rows), F32),

time: 114 us -> 102 us (0.89)
  Pallas kernels: 95.8 us -> 87.7 us
  local copies, waits for them, and re-layouts: 10.2 us -> 7.29 us
    pallas_call x1, Pallas kernels: 59.3 us -> 50.4 us  [body(): pl.pallas_call(functools.partial(attend_kernel, nz, nx, ntp, heads), out_...]
    concatenate x2 -> x0, local copies, waits for them, and re-layouts: 1.62 us -> none  [the longest x1 0.81 us: body(): cos_full = jnp.concatenate([cosine, cosine], axis=1)]
    unnamed x21 -> x24, local copies, waits for them, and re-layouts: 5.56 us -> 4.24 us
  transfers between devices with their start and end apart: 1 -> 1, of which waited for: 0 -> 0; matrix products, arithmetic and copies ran while one was open for 3% -> 3% of each run, Pallas kernels for 53% -> 50%
where the time goes in v2:
time: 102 us; the launch traced here: 101 us
  Pallas kernels  87.7 us (86%)
  local copies, waits for them, and re-layouts  7.29 us (7%)
  other arithmetic  2.51 us (2%)
  matrix products  1.69 us (2%)
  starting transfers between devices  1.28 us (1%)
    pallas_call x1, Pallas kernels, body(): pl.pallas_call(functools.partial(attend_kernel, nz, nx, ntp, heads), out_...  50.4 us
    pallas_call x1, Pallas kernels, body(): pl.pallas_call(functools.partial(finish_kernel, ntp, chunk), out_shape=st...  20.5 us
    pallas_call x1, Pallas kernels, body(): pl.pallas_call(functools.partial(project_kernel, ntp, chunk), out_shape=[...  16.8 us
    unnamed x24, local copies, waits for them, and re-layouts  4.24 us
  transfers between devices with their start and end apart: 1, of which 0 were waited for; matrix products, arithmetic and copies ran while one was open for 3% of the time, Pallas kernels for 50%

profile of v2, /device:TPU:27, one launch (start us, length us, event | category | flops | bytes accessed | tf_op | source)
XLA Modules:
  0.0 101.3 jit_solution(9999781166171826950)
XLA Ops:
  0.6 0.0 copy-start
  0.7 1.4 %broadcast_in_dim.26.qg = f32[1,768]{1,0:T(1,128)} reshape(f32[768]{0:T(1024)} %param.23) | data formatting | bytes 6144 | tf_op jit(solution)/shard_map/broadcast_in_dim | solution.py:479
  2.0 0.2 fusion.4
  2.2 0.6 copy-done.2
  2.8 0.6 pad_maximum_fusion.1
  3.5 0.0 copy-done.4
  3.5 16.8 %project.1 = (bf16[384,256]{1,0:T(8,128)(2,1)}, bf16[384,256]{1,0:T(8,128)(2,1)}, bf16[384,768]{1,0:T(8,128)(2,1)}, bf16[384,640]{1,0:T(8,128)(2,1)}) custom-call(bf16[384,512]{1,0:T(8,128)(2,1)} %tok.1, f32[1,2048]{1,0:T(1,128)} %bitcast.16, f32[1,768]{1,0:T(1,128)} %broadcast_in_dim.26.qg, f32[1,512]{1,0:T(1,128)} %bitcast.21, ...), custom_call_target="tpu_custom_call" | custom-call | tf_op jit(solution)/shard_map/project/pallas_call | solution.py:462
  20.3 1.2 %slice.32 = bf16[2,256]{1,0:T(2,128)(2,1)} slice(bf16[384,256]{1,0:T(8,128)(2,1)} %get-tuple-element.12), slice={[382:384], [0:256]} | slice | bytes 2048 | tf_op jit(solution)/shard_map/slice | solution.py:513
  21.5 1.3 %collective-permute-start = (bf16[2,256]{1,0:T(2,128)(2,1)}, bf16[2,256]{1,0:T(2,128)(2,1)S(1)}, u32[]{:S(2)}, u32[]{:S(2)}) collective-permute-start(bf16[2,256]{1,0:T(2,128)(2,1)} %slice.32), channel_id=1, source_target_pairs={{0,4},{4,8},{8,12},{12,16},{16,20},{20,24},{24,28},{1,5},{5,9},{9,... | collective-permute-start | bytes 3080 | tf_op jit(solution)/shard_map/ppermute | solution.py:513
  22.9 1.7 %convolution_bitcast_fusion = f32[768,384]{0,1:T(8,128)S(1)} fusion(bf16[384,768]{1,0:T(8,128)(2,1)} %get-tuple-element.9, bf16[768,768]{1,0:T(8,128)(2,1)S(1)} %copy-done), kind=kOutput, calls=%fused_computation | convolution fusion | flops 452984832 | bytes 2949120 | tf_op jit(solution)/shard_map/dot_general | solution.py:482
  24.6 0.4 copy.18
  25.0 0.1 broadcast_dynamic-update-slice_fusion.1
  25.1 0.8 fusion.2
  25.9 0.1 broadcast_dynamic-update-slice_fusion.qt
  26.0 0.0 copy-start.1
  26.0 0.0 copy-start.6
  26.0 0.0 copy-start.7
  26.1 1.1 %copy-done.1 = bf16[8,256,384]{2,1,0:T(8,128)(2,1)} copy-done((bf16[8,256,384]{2,1,0:T(8,128)(2,1)}, bf16[8,256,384]{2,1,0:T(8,128)(2,1)S(1)}, u32[]{:S(2)}) %copy-start.1) | copy-done | bytes 1572888
  27.2 50.4 %attend.1 = (bf16[384,512]{1,0:T(8,128)(2,1)}, f32[8,384]{1,0:T(8,128)}) custom-call(bf16[384,640]{1,0:T(8,128)(2,1)} %get-tuple-element.8.kvb, bf16[8,256,384]{2,1,0:T(8,128)(2,1)} %copy-done.1, bf16[512,1024]{1,0:T(8,128)(2,1)} %up.1), custom_call_target="tpu_custom_call" | custom-call | tf_op jit(solution)/shard_map/attend/pallas_call | solution.py:496
  77.6 0.0 collective-permute-done
  77.6 0.8 multiply_convert_fusion.conv
  78.5 20.5 %finish.1 = bf16[384,512]{1,0:T(8,128)(2,1)} custom-call(bf16[384,512]{1,0:T(8,128)(2,1)} %get-tuple-element.10.att, bf16[384,256]{1,0:T(8,128)(2,1)} %multiply_convert_fusion.conv, bf16[512,2048]{1,0:T(8,128)(2,1)} %wa.1, bf16[256,2048]{1,0:T(8,128)(2,1)} %wc.1, f32[1,512]{1,0:T(1,128)} %bitcast.20), custom_call_target="tpu_custom_call" | custom-call | tf_op jit(solution)/shard_map/finish/pallas_call | solution.py:523
  99.0 1.8 %copy.25 = bf16[384,512]{1,0:T(8,128)(2,1)} copy(bf16[384,512]{1,0:T(8,128)(2,1)} %finish.1) | data formatting | bytes 786432
  100.7 0.6 copy.26
  (18 shorter events, 0.1 us)
Async XLA Ops:
  0.6 22.2 %copy-start = (bf16[768,768]{1,0:T(8,128)(2,1)S(1)}, bf16[768,768]{1,0:T(8,128)(2,1)}, u32[]{:S(2)}) copy-start(bf16[768,768]{1,0:T(8,128)(2,1)} %param.24) | copy-start | bytes 3538948
  2.2 0.6 copy-start.2
  2.2 1.2 %copy-start.4 = (f32[16,384]{1,0:T(8,128)}, f32[16,384]{1,0:T(8,128)S(1)}, u32[]{:S(2)}) copy-start(f32[16,384]{1,0:T(8,128)S(1)} %get-tuple-element.16) | copy-start | bytes 73732
  3.5 19.4 %copy-start.9 = (bf16[3,256]{1,0:T(4,128)(2,1)S(1)}, bf16[3,256]{1,0:T(4,128)(2,1)}, u32[]{:S(2)}) copy-start(bf16[3,256]{1,0:T(4,128)(2,1)} %param.21) | copy-start | bytes 4612
  21.5 56.1 %collective-permute-start = (bf16[2,256]{1,0:T(2,128)(2,1)}, bf16[2,256]{1,0:T(2,128)(2,1)S(1)}, u32[]{:S(2)}, u32[]{:S(2)}) collective-permute-start(bf16[2,256]{1,0:T(2,128)(2,1)} %slice.32), channel_id=1, source_target_pairs={{0,4},{4,8},{8,12},{12,16},{16,20},{20,24},{24,28},{1,5},{5,9},{9,... | collective-permute-start | bytes 3080 | tf_op jit(solution)/shard_map/ppermute | solution.py:513
  24.9 0.9 copy-start.3
  24.9 0.9 copy-start.5
  26.0 1.2 %copy-start.1 = (bf16[8,256,384]{2,1,0:T(8,128)(2,1)}, bf16[8,256,384]{2,1,0:T(8,128)(2,1)S(1)}, u32[]{:S(2)}) copy-start(bf16[8,256,384]{2,1,0:T(8,128)(2,1)S(1)} %broadcast_dynamic-update-slice_fusion.qt) | copy-start | bytes 4718596
  26.0 51.6 %copy-start.6 = (bf16[384,256]{1,0:T(8,128)(2,1)S(1)}, bf16[384,256]{1,0:T(8,128)(2,1)}, u32[]{:S(2)}) copy-start(bf16[384,256]{1,0:T(8,128)(2,1)} %get-tuple-element.12) | copy-start | bytes 589828
  26.0 51.6 %copy-start.7 = (bf16[384,256]{1,0:T(8,128)(2,1)S(1)}, bf16[384,256]{1,0:T(8,128)(2,1)}, u32[]{:S(2)}) copy-start(bf16[384,256]{1,0:T(8,128)(2,1)} %get-tuple-element.11) | copy-start | bytes 589828
  78.5 22.3 %copy-start.8 = (f32[8,384]{1,0:T(8,128)S(1)}, f32[8,384]{1,0:T(8,128)}, u32[]{:S(2)}) copy-start(f32[8,384]{1,0:T(8,128)} %get-tuple-element.25) | copy-start | bytes 36868
